TPU v7x, 32 devices: a whole 2x2x4 slice. The times are simulated.
32 devices in a mesh: ep: 8 (over z, y), tp: 4 (over x, core).
Axes of the slice: x: 2, y: 2, z: 4, core: 2. Of those that a mesh axis runs over, the one named last changes fastest.
Arguments:
- tokens: bfloat16 [6144, 2048], P('ep', 'tp')
- norm_gain: float32 [2048], P('tp'), may hold values from 0.1 to 1.9
- routing: int32 [6144, 2], P('ep'), may hold values from 0 to 7, as said below
- route_weight: float32 [6144, 2], P('ep'), may hold values from 0.2 to 1
- w_gate: bfloat16 [8, 2048, 512], P('ep', 'tp'), may hold values from -0.125 to 0.125
- w_up: bfloat16 [8, 2048, 512], P('ep', 'tp'), may hold values from -0.125 to 0.125
- w_down: bfloat16 [8, 512, 2048], P('ep', None, 'tp'), may hold values from -0.25 to 0.25
- w_branch_in: bfloat16 [2048, 1024], P('ep', 'tp'), may hold values from -0.125 to 0.125
- w_branch_out: bfloat16 [1024, 2048], P('tp', 'ep'), may hold values from -0.1875 to 0.1875
- branch_gate: float32 [2048], P('tp'), may hold values from -3 to 3
Outputs:
- mixed: bfloat16 [6144, 2048], P('ep', 'tp')
Inputs may be any that keep to these rules, and one draw needn't show every extreme that they name: `routing`: each row names two different experts of the same group; expert e belongs to group e // 2. Among the rows of one device (aligned blocks of 768 rows) no expert is named more than 384 times, and in every block all experts of one group are named exactly 384 times.
All inputs are finite; a program needn't handle non-finite values.
Results may differ from a plain program's by a relative error of at most 0.0069.
Values may be sent and summed in bfloat16 or wider, within the bound.
A program may use at most 128 MiB of HBM per device.

v0:
```python
import jax
import jax.numpy as jnp
from jax import lax
from jax.sharding import PartitionSpec as P

GROUPS = 4
epsilon = 1e-06


def send_back(result):
    return lax.all_to_all(result, "ep", split_axis=0, concat_axis=0, tiled=True)


def body(
    tokens,
    norm_gain,
    routing,
    route_weight,
    w_gate,
    w_up,
    w_down,
    w_branch_in,
    w_branch_out,
    branch_gate,
):
    token_count, quarter = tokens.shape
    full_width = quarter * lax.axis_size("tp")
    floats = tokens.astype(jnp.float32)
    squares = lax.psum(jnp.sum(floats * floats, axis=1), "tp")
    normed = (floats * lax.rsqrt(squares[:, None] / full_width + epsilon) * norm_gain).astype(
        jnp.bfloat16
    )
    expert_count = lax.axis_size("ep") * w_gate.shape[0]
    capacity = token_count // (expert_count // GROUPS)
    flat_ids = routing.reshape(-1)
    one_hot = (flat_ids[:, None] == jnp.arange(expert_count, dtype=jnp.int32)[None, :]).astype(
        jnp.int32
    )
    before = jnp.cumsum(one_hot, axis=0) - one_hot
    position = flat_ids * capacity + jnp.sum(before * one_hot, axis=1)
    copies = jnp.repeat(normed, 2, axis=0)
    buffer = jnp.zeros((expert_count * capacity, quarter), jnp.bfloat16).at[position].set(copies)
    buffer = buffer.reshape(expert_count, capacity, quarter)
    gate_whole, up_whole, down_whole = (
        lax.all_gather(w_gate[0], "tp", axis=0, tiled=True),
        lax.all_gather(w_up[0], "tp", axis=0, tiled=True),
        lax.all_gather(w_down[0], "tp", axis=1, tiled=True),
    )
    row_split = lax.all_to_all(
        lax.all_to_all(buffer, "ep", split_axis=0, concat_axis=0, tiled=True),
        "tp",
        split_axis=0,
        concat_axis=2,
        tiled=True,
    )
    slot_rows = row_split.reshape(-1, row_split.shape[2])
    gate_sum = jnp.dot(slot_rows, gate_whole, preferred_element_type=jnp.float32)
    up_sum = jnp.dot(slot_rows, up_whole, preferred_element_type=jnp.float32)
    hidden = (jax.nn.silu(gate_sum) * up_sum).astype(jnp.bfloat16)
    result = jnp.dot(hidden, down_whole, preferred_element_type=jnp.float32).astype(jnp.bfloat16)
    feature_split = lax.all_to_all(
        result.reshape(row_split.shape), "tp", split_axis=2, concat_axis=0, tiled=True
    )
    returned = send_back(feature_split)
    picked = returned.reshape(expert_count * capacity, quarter)[position].reshape(
        token_count, 2, quarter
    )
    routed = jnp.sum(picked.astype(jnp.float32) * route_weight[:, :, None], axis=1)
    branch_tokens = lax.all_to_all(normed, "tp", split_axis=0, concat_axis=1, tiled=True)
    in_cols, out_rows = (
        lax.all_gather(w_branch_in, "tp", axis=1, tiled=True),
        lax.all_gather(w_branch_out, "tp", axis=0, tiled=True),
    )
    in_whole, out_whole = (
        lax.all_gather(in_cols, "ep", axis=0, tiled=True),
        lax.all_gather(out_rows, "ep", axis=1, tiled=True),
    )
    branch_hidden = jax.nn.silu(
        jnp.dot(branch_tokens, in_whole, preferred_element_type=jnp.float32)
    ).astype(jnp.bfloat16)
    branch_local = jnp.dot(branch_hidden, out_whole, preferred_element_type=jnp.float32).astype(
        jnp.bfloat16
    )
    branch = lax.all_to_all(branch_local, "tp", split_axis=1, concat_axis=0, tiled=True)
    return (routed + jax.nn.sigmoid(branch_gate) * branch.astype(jnp.float32)).astype(jnp.bfloat16)


def solution(mesh):
    return jax.shard_map(
        body,
        mesh=mesh,
        in_specs=(
            P("ep", "tp"),
            P("tp"),
            P("ep", None),
            P("ep", None),
            P("ep", "tp", None),
            P("ep", "tp", None),
            P("ep", None, "tp"),
            P("ep", "tp"),
            P("tp", "ep"),
            P("tp"),
        ),
        out_specs=P("ep", "tp"),
        check_vma=False,
    )
```

profile of v0, /device:TPU:0, one launch (start us, length us, event | category | flops | bytes accessed | tf_op | source)
XLA Modules:
  0.0 403.0 jit_solution(17927686198045265100)
XLA Ops:
  6.5 0.7 all-gather.13.cloned.1.call-update
  7.3 0.0 all-gather.15.cloned.1.call-start
  7.3 0.7 all-gather.15.cloned.1.call-update
  8.1 0.7 all-gather.17.cloned.1.call-update
  8.8 0.9 copy.30
  9.6 0.7 broadcast_multiply_fusion
  10.3 0.2 eq.29
  10.6 0.2 fusion.5
  10.8 8.4 %psum.7 = f32[768]{0:T(1024)S(1)} all-reduce(f32[768]{0:T(1024)S(1)} %fusion.5), channel_id=1, replica_groups=mesh['ep'=8,'tp'=4] {'tp'}, use_global_device_ids=true, to_apply=%region_4.5 | all-reduce | flops 768 | bytes 6144 | tf_op jit(solution)/shard_map/psum | solution.py:29
  19.2 2.3 reduce-window.6
  21.5 0.3 slice_reduce_fusion
  21.7 0.2 eq.25
  22.0 0.2 reduce-window.9
  22.1 0.2 copy.29
  22.3 0.3 mul.67
  22.6 0.2 fusion.7
  22.9 0.9 copy-done
  23.7 0.8 broadcast_in_dim.5
  24.5 0.6 reshape.100
  25.2 0.1 add_bitcast_fusion
  25.4 9.5 %scatter_custom_fusion = bf16[3072,512]{1,0:T(8,128)(2,1)} fusion(s32[1536]{0:T(1024)S(1)} %fusion.21, bf16[1536,512]{1,0:T(8,128)(2,1)S(1)} %reshape.100, bf16[]{:T(256)} %constant.8.clone.1), kind=kCustom, calls=%fused_computation.19 | custom fusion | bytes 3145730 | tf_op jit(solution)/shard_map/scatter | solution.py:42
  34.8 6.0 %all-to-all-start = ((bf16[8,384,512]{2,1,0:T(8,128)(2,1)}), bf16[8,384,512]{2,1,0:T(8,128)(2,1)S(1)}, u32[]{:S(2)}, u32[]{:S(2)}) async-start(bf16[8,384,512]{2,1,0:T(8,128)(2,1)} %bitcast.69), calls=%async_computation | async-start | bytes 6291456 | tf_op jit(solution)/shard_map/all_to_all | solution.py:50
  40.8 8.6 %all_gather.26 = bf16[1024,256]{1,0:T(8,128)(2,1)} all-gather(bf16[256,256]{1,0:T(8,128)(2,1)S(1)} %copy-done.2), channel_id=1, replica_groups=mesh['ep'=8,'tp'=4] {'tp'}, dimensions={0}, use_global_device_ids=true | all-gather | bytes 655360 | tf_op jit(solution)/shard_map/all_gather | solution.py:72
  49.5 75.0 %all-to-all-done = bf16[8,384,512]{2,1,0:T(8,128)(2,1)S(1)} async-done(((bf16[8,384,512]{2,1,0:T(8,128)(2,1)}), bf16[8,384,512]{2,1,0:T(8,128)(2,1)S(1)}, u32[]{:S(2)}, u32[]{:S(2)}) %all-to-all-start) | async-done | bytes 3145760 | tf_op jit(solution)/shard_map/all_to_all | solution.py:50
  124.5 39.5 %all_to_all.75 = bf16[8,384,512]{2,1,0:T(8,128)(2,1)S(1)} all-to-all(bf16[8,384,512]{2,1,0:T(8,128)(2,1)S(1)} %all-to-all-done), channel_id=1, replica_groups=mesh['ep'=8,'tp'=4] {'tp'}, dimensions={0} | all-to-all | bytes 6291456 | tf_op jit(solution)/shard_map/all_to_all | solution.py:49
  164.0 2.4 copy.32
  166.4 1.0 copy.41
  167.5 4.5 %fusion.3 = f32[768,512]{1,0:T(8,128)} fusion(bf16[768,2048]{1,0:T(8,128)(2,1)S(1)} %bitcast.73, bf16[1,2048,512]{2,1,0:T(8,128)(2,1)} %all-gather.13.cloned.1.call-done), kind=kOutput, calls=%fused_computation.8 | convolution fusion | flops 1610612736 | bytes 6815744 | tf_op jit(solution)/shard_map/dot_general | solution.py:57
  172.0 7.9 %convolution_convert_fusion = bf16[768,2048]{1,0:T(8,128)(2,1)} fusion(bf16[1,512,2048]{2,1,0:T(8,128)(2,1)} %all-gather.17.cloned.1.call-done, f32[768,512]{1,0:T(8,128)} %fusion.3, bf16[768,2048]{1,0:T(8,128)(2,1)S(1)} %bitcast.74, bf16[1,2048,512]{2,1,0:T(8,128)(2,1)} %all-gather.15.cloned.1.call-done), kind=kOutput, calls=%fused_computation.2 | convolution fusion | flops 3225157632 | bytes 12058624 | tf_op jit(solution)/shard_map/dot_general | solution.py:60
  179.9 8.8 %copy.33 = bf16[2,384,2048]{1,0,2:T(2,128)(2,1)} copy(bf16[2,384,2048]{2,1,0:T(8,128)(2,1)} %bitcast.75) | data formatting | bytes 6291456 | tf_op jit(solution)/shard_map/reshape | solution.py:62
  188.6 3.8 all-to-all-start.2
  192.5 0.0 all-gather.9.cloned.1.call-start
  192.5 40.9 %all_gather.24 = bf16[256,1024]{1,0:T(8,128)(2,1)} all-gather(bf16[256,256]{1,0:T(8,128)(2,1)S(1)} %copy-done.3), channel_id=1, replica_groups=mesh['ep'=8,'tp'=4] {'tp'}, dimensions={1}, use_global_device_ids=true | all-gather | bytes 655360 | tf_op jit(solution)/shard_map/all_gather | solution.py:71
  233.5 4.2 %all-to-all-start.4 = ((bf16[4,192,512]{2,1,0:T(8,128)(2,1)}), bf16[4,192,512]{2,1,0:T(8,128)(2,1)}, u32[]{:S(2)}, u32[]{:S(2)}) async-start(bf16[4,192,512]{2,1,0:T(8,128)(2,1)} %bitcast.72), calls=%async_computation.4 | async-start | bytes 1572864 | tf_op jit(solution)/shard_map/all_to_all | solution.py:69
  237.7 6.7 %copy.34 = bf16[4,2,384,512]{3,2,1,0:T(8,128)(2,1)} copy(bf16[4,2,384,512]{2,1,3,0:T(2,128)(2,1)S(1)} %bitcast.68) | data formatting | bytes 6291456 | tf_op jit(solution)/shard_map/all_to_all | solution.py:61
  244.4 5.0 %all-to-all-done.4 = bf16[4,192,512]{2,1,0:T(8,128)(2,1)} async-done(((bf16[4,192,512]{2,1,0:T(8,128)(2,1)}), bf16[4,192,512]{2,1,0:T(8,128)(2,1)}, u32[]{:S(2)}, u32[]{:S(2)}) %all-to-all-start.4) | async-done | bytes 786464 | tf_op jit(solution)/shard_map/all_to_all | solution.py:69
  249.4 6.3 %all-to-all-start.3 = ((bf16[8,384,512]{2,1,0:T(8,128)(2,1)}), bf16[8,384,512]{2,1,0:T(8,128)(2,1)S(1)}, u32[]{:S(2)}, u32[]{:S(2)}) async-start(bf16[8,384,512]{2,1,0:T(8,128)(2,1)} %bitcast.67), calls=%async_computation.3 | async-start | bytes 6291456 | tf_op jit(solution)/shard_map/all_to_all | solution.py:11
  255.7 2.1 copy.39
  257.8 107.4 %all-gather.9.cloned.1.call-done = bf16[2048,1024]{1,0:T(8,128)(2,1)} async-done(((bf16[256,1024]{1,0:T(8,128)(2,1)}), bf16[2048,1024]{1,0:T(8,128)(2,1)}) %all-gather.9.cloned.1.call-update) | async-done | bytes 4194320 | tf_op jit(solution)/shard_map/all_gather | solution.py:75
  365.2 6.4 %convolution_convert_fusion.1 = bf16[192,2048]{1,0:T(8,128)(2,1)} fusion(bf16[1024,2048]{1,0:T(8,128)(2,1)} %all-gather.11.cloned.1.call-done, bf16[192,2048]{1,0:T(8,128)(2,1)} %bitcast.77, bf16[2048,1024]{1,0:T(8,128)(2,1)} %all-gather.9.cloned.1.call-done), kind=kOutput, calls=%fused_computation.4 | convolution fusion | flops 1611988992 | bytes 9961472 | tf_op jit(solution)/shard_map/dot_general | solution.py:81
  371.7 2.1 copy.44
  373.8 4.4 %all-to-all-start.5 = ((bf16[192,4,512]{2,0,1:T(8,128)(2,1)}), bf16[192,4,512]{2,0,1:T(8,128)(2,1)}, u32[]{:S(2)}, u32[]{:S(2)}) async-start(bf16[192,4,512]{2,0,1:T(8,128)(2,1)} %bitcast.76), calls=%async_computation.5 | async-start | bytes 1572864 | tf_op jit(solution)/shard_map/all_to_all | solution.py:84
  378.2 0.6 add_divide_fusion
  378.8 0.2 copy.35
  379.0 5.4 %gather_fusion = bf16[1536,512]{1,0:T(8,128)(2,1)} fusion(bf16[3072,512]{1,0:T(8,128)(2,1)S(1)} %bitcast.66, s32[2048]{0:T(1024)S(1)} %pad_clamp_fusion), kind=kCustom, calls=%fused_computation | custom fusion | bytes 3151872 | tf_op jit(solution)/shard_map/gather | solution.py:65
  384.4 3.4 reshape.86
  387.8 5.9 %multiply_reduce_fusion = f32[768,512]{1,0:T(8,128)} fusion(f32[768,2,512]{2,1,0:T(2,128)S(1)} %reshape.86, f32[768,2]{1,0:T(8,128)S(1)} %copy.35), kind=kLoop, calls=%fused_computation.3 | loop fusion | flops 1179648 | bytes 4724736 | tf_op jit(solution)/shard_map/reduce_sum | solution.py:68
  393.8 2.7 fusion.9
  (32 shorter events, 0.3 us)
Async XLA Ops:
  6.5 4.0 %copy-start.1 = (bf16[768,512]{1,0:T(8,128)(2,1)S(1)}, bf16[768,512]{1,0:T(8,128)(2,1)}, u32[]{:S(2)}) copy-start(bf16[768,512]{1,0:T(8,128)(2,1)} %param.10) | copy-start | bytes 2359300
  6.5 160.9 %all-gather.13.cloned.1.call-start = ((), (), s32[]{:S(2)}) async-start(), calls=%async_computation.8 | async-start | bytes 2621440 | tf_op jit(solution)/shard_map/all_gather | solution.py:45
  7.3 15.3 %copy-start.6 = (f32[512]{0:T(512)S(1)}, f32[512]{0:T(512)}, u32[]{:S(2)}) copy-start(f32[512]{0:T(512)} %param.11) | copy-start | bytes 6148
  7.3 164.7 %all-gather.15.cloned.1.call-start = ((), (), s32[]{:S(2)}) async-start(), calls=%async_computation.9 | async-start | bytes 2621440 | tf_op jit(solution)/shard_map/all_gather | solution.py:46
  8.0 164.0 %all-gather.17.cloned.1.call-start = ((), (), s32[]{:S(2)}) async-start(), calls=%async_computation.10 | async-start | bytes 2621440 | tf_op jit(solution)/shard_map/all_gather | solution.py:47
  22.9 0.9 copy-start
  34.8 6.0 %copy-start.2 = (bf16[256,256]{1,0:T(8,128)(2,1)S(1)}, bf16[256,256]{1,0:T(8,128)(2,1)}, u32[]{:S(2)}) copy-start(bf16[256,256]{1,0:T(8,128)(2,1)} %param.18) | copy-start | bytes 393220
  34.8 89.7 %all-to-all-start = ((bf16[8,384,512]{2,1,0:T(8,128)(2,1)}), bf16[8,384,512]{2,1,0:T(8,128)(2,1)S(1)}, u32[]{:S(2)}, u32[]{:S(2)}) async-start(bf16[8,384,512]{2,1,0:T(8,128)(2,1)} %bitcast.69), calls=%async_computation | async-start | bytes 6291456 | tf_op jit(solution)/shard_map/all_to_all | solution.py:50
  40.8 217.0 %all-gather.11.cloned.1.call-start = ((), (), s32[]{:S(2)}) async-start(), calls=%async_computation.7 | async-start | bytes 4718592 | tf_op jit(solution)/shard_map/all_gather | solution.py:76
  188.6 3.9 copy-start.3
  188.6 44.9 %all-to-all-start.2 = ((bf16[2,384,2048]{1,0,2:T(2,128)(2,1)}), bf16[2,384,2048]{1,0,2:T(2,128)(2,1)S(1)}, u32[]{:S(2)}, u32[]{:S(2)}) async-start(bf16[2,384,2048]{1,0,2:T(2,128)(2,1)} %copy.33), calls=%async_computation.2 | async-start | bytes 6291456 | tf_op jit(solution)/shard_map/all_to_all | solution.py:61
  192.5 172.7 %all-gather.9.cloned.1.call-start = ((), (), s32[]{:S(2)}) async-start(), calls=%async_computation.6 | async-start | bytes 4718592 | tf_op jit(solution)/shard_map/all_gather | solution.py:75
  233.5 15.9 %all-to-all-start.4 = ((bf16[4,192,512]{2,1,0:T(8,128)(2,1)}), bf16[4,192,512]{2,1,0:T(8,128)(2,1)}, u32[]{:S(2)}, u32[]{:S(2)}) async-start(bf16[4,192,512]{2,1,0:T(8,128)(2,1)} %bitcast.72), calls=%async_computation.4 | async-start | bytes 1572864 | tf_op jit(solution)/shard_map/all_to_all | solution.py:69
  249.4 124.4 %all-to-all-start.3 = ((bf16[8,384,512]{2,1,0:T(8,128)(2,1)}), bf16[8,384,512]{2,1,0:T(8,128)(2,1)S(1)}, u32[]{:S(2)}, u32[]{:S(2)}) async-start(bf16[8,384,512]{2,1,0:T(8,128)(2,1)} %bitcast.67), calls=%async_computation.3 | async-start | bytes 6291456 | tf_op jit(solution)/shard_map/all_to_all | solution.py:11
  371.7 6.6 %copy-start.7 = (f32[512]{0:T(512)S(1)}, f32[512]{0:T(512)}, u32[]{:S(2)}) copy-start(f32[512]{0:T(512)} %param.19) | copy-start | bytes 6148
  371.7 7.2 %copy-start.5 = (f32[768,2]{0,1:T(2,128)S(1)}, f32[768,2]{0,1:T(2,128)}, u32[]{:S(2)}) copy-start(f32[768,2]{0,1:T(2,128)} %param.13) | copy-start | bytes 18436
  373.8 20.0 %all-to-all-start.5 = ((bf16[192,4,512]{2,0,1:T(8,128)(2,1)}), bf16[192,4,512]{2,0,1:T(8,128)(2,1)}, u32[]{:S(2)}, u32[]{:S(2)}) async-start(bf16[192,4,512]{2,0,1:T(8,128)(2,1)} %bitcast.76), calls=%async_computation.5 | async-start | bytes 1572864 | tf_op jit(solution)/shard_map/all_to_all | solution.py:84
  387.8 5.9 %copy-start.4 = (f32[512]{0:T(512)S(1)}, f32[512]{0:T(512)}, u32[]{:S(2)}) copy-start(f32[512]{0:T(512)} %add_divide_fusion) | copy-start | bytes 6148
Sparse Core Ops, SparseCore 0:
  8.9 25.2 all-gather.12
  35.8 23.4 all-gather.14
  60.8 23.6 all-gather.16
  86.4 92.0 all-gather.10
  233.6 131.5 all-gather.8
where the time goes:
time: 404 us; the launch traced here: 403 us
  waiting for transfers between devices  190 us (47%)
  blocking collectives  97.4 us (24%)
  local copies, waits for them, and re-layouts  46 us (11%)
  starting transfers between devices  24.9 us (6%)
  matrix products  18.9 us (5%)
  between operations  13.4 us (3%)
  other arithmetic  13 us (3%)
    all_gather x1, waiting for transfers between devices, body(): lax.all_gather(in_cols, 'ep', axis=0, tiled=True)  107 us
    all_to_all x1, waiting for transfers between devices, body(): lax.all_to_all(buffer, 'ep', split_axis=0, concat_axis=0, tiled=True)  75 us
    all_gather x1, blocking collectives, body(): lax.all_gather(w_branch_in, 'tp', axis=1, tiled=True)  40.9 us
    all_to_all x1, blocking collectives, body(): lax.all_to_all(lax.all_to_all(buffer, 'ep', split_axis=0, concat_axis=0,...  39.5 us
    scatter x1, local copies, waits for them, and re-layouts, body(): jnp.zeros((expert_count * capacity, quarter), jnp.bfloat16).at[position]  9.46 us
    reshape x1, local copies, waits for them, and re-layouts, body(): result.reshape(row_split.shape)  8.75 us
    all_gather x1, blocking collectives, body(): lax.all_gather(w_branch_out, 'tp', axis=0, tiled=True)  8.6 us
    psum x1, blocking collectives, body(): squares = lax.psum(jnp.sum(floats * floats, axis=1), 'tp')  8.37 us
  transfers between devices with their start and end apart: 10, of which 3 were waited for; matrix products, arithmetic and copies ran while one was open for 18% of the time, Pallas kernels for 0%

commit v1 on v0

--- a/solution.py
+++ b/solution.py
@@ -23,6 +23,16 @@
     w_branch_out,
     branch_gate,
 ):
+
+    def _spread_face(packet):
+        response = jax.lax.all_to_all(
+            jnp.stack([packet for _ in range(jax.lax.psum(1, axis_name="tp"))], axis=0),
+            axis_name="tp",
+            split_axis=0,
+            concat_axis=0,
+        )
+        return jnp.concatenate(response, 1)
+
     token_count, quarter = tokens.shape
     full_width = quarter * lax.axis_size("tp")
     floats = tokens.astype(jnp.float32)
@@ -68,7 +78,7 @@
     routed = jnp.sum(picked.astype(jnp.float32) * route_weight[:, :, None], axis=1)
     branch_tokens = lax.all_to_all(normed, "tp", split_axis=0, concat_axis=1, tiled=True)
     in_cols, out_rows = (
-        lax.all_gather(w_branch_in, "tp", axis=1, tiled=True),
+        _spread_face(w_branch_in),
         lax.all_gather(w_branch_out, "tp", axis=0, tiled=True),
     )
     in_whole, out_whole = (

time: 404 us -> 374 us (0.926)
  blocking collectives: 97.4 us -> 17.1 us
  waiting for transfers between devices: 190 us -> 230 us
  starting transfers between devices: 24.9 us -> 32.7 us
    all_gather x1, waiting for transfers between devices: 107 us -> 41.1 us  [body(): lax.all_gather(in_cols, 'ep', axis=0, tiled=True)]
    all_gather x1 -> x0, blocking collectives: 40.9 us -> none  [body(): lax.all_gather(w_branch_in, 'tp', axis=1, tiled=True)]
    all_to_all x1 -> x0, blocking collectives: 39.5 us -> none  [body(): lax.all_to_all(lax.all_to_all(buffer, 'ep', split_axis=0, concat_axis=0,...]
    all_to_all x0 -> x2, waiting for transfers between devices: none -> 36.8 us  [the longest x1 36.8 us: body(): lax.all_to_all(lax.all_to_all(buffer, 'ep', split_axis=0, concat_axis=0,...]
    all_to_all x1, waiting for transfers between devices: 0.01 us -> 36.3 us  [body(): lax.all_to_all(result.reshape(row_split.shape), 'tp', split_axis=2, conca...]
    all_to_all x1, waiting for transfers between devices: 0.01 us -> 33.7 us  [send_back(): return lax.all_to_all(result, 'ep', split_axis=0, concat_axis=0, tiled=True)]
    all_to_all x0 -> x2, starting transfers between devices: none -> 8.03 us  [the longest x1 4.31 us: _spread_face(): jax.lax.all_to_all(jnp.stack([packet for _ in range(jax.lax.psum(1, axis_...]
  transfers between devices with their start and end apart: 10 -> 12, of which waited for: 3 -> 6; matrix products, arithmetic and copies ran while one was open for 18% -> 20% of each run, Pallas kernels for 0% -> 0%
where the time goes in v1:
time: 374 us; the launch traced here: 373 us
  waiting for transfers between devices  230 us (61%)
  local copies, waits for them, and re-layouts  47.1 us (13%)
  starting transfers between devices  32.7 us (9%)
  matrix products  19.5 us (5%)
  blocking collectives  17.1 us (5%)
  between operations  13.4 us (4%)
  other arithmetic  13 us (3%)
    all_to_all x1, waiting for transfers between devices, body(): lax.all_to_all(buffer, 'ep', split_axis=0, concat_axis=0, tiled=True)  75 us
    all_gather x1, waiting for transfers between devices, body(): lax.all_gather(in_cols, 'ep', axis=0, tiled=True)  41.1 us
    all_to_all x1, waiting for transfers between devices, body(): lax.all_to_all(lax.all_to_all(buffer, 'ep', split_axis=0, concat_axis=0,...  36.8 us
    all_to_all x1, waiting for transfers between devices, body(): lax.all_to_all(result.reshape(row_split.shape), 'tp', split_axis=2, conca...  36.3 us
    all_to_all x1, waiting for transfers between devices, send_back(): return lax.all_to_all(result, 'ep', split_axis=0, concat_axis=0, tiled=True)  33.7 us
    scatter x1, local copies, waits for them, and re-layouts, body(): jnp.zeros((expert_count * capacity, quarter), jnp.bfloat16).at[position]  9.5 us
    reshape x1, local copies, waits for them, and re-layouts, body(): result.reshape(row_split.shape)  8.85 us
    all_gather x1, blocking collectives, body(): lax.all_gather(w_branch_out, 'tp', axis=0, tiled=True)  8.69 us
  transfers between devices with their start and end apart: 12, of which 6 were waited for; matrix products, arithmetic and copies ran while one was open for 20% of the time, Pallas kernels for 0%

profile of v1, /device:TPU:0, one launch (start us, length us, event | category | flops | bytes accessed | tf_op | source)
XLA Modules:
  0.0 373.3 jit_solution(15003782295661667089)
XLA Ops:
  6.5 0.7 all-gather.13.cloned.1.call-update
  7.3 0.7 all-gather.15.cloned.1.call-update
  8.1 0.7 all-gather.17.cloned.1.call-update
  8.8 0.9 copy.32
  9.6 0.7 broadcast_multiply_fusion
  10.3 0.2 eq.29
  10.6 0.2 fusion.5
  10.8 8.4 %psum.7 = f32[768]{0:T(1024)S(1)} all-reduce(f32[768]{0:T(1024)S(1)} %fusion.5), channel_id=1, replica_groups=mesh['ep'=8,'tp'=4] {'tp'}, use_global_device_ids=true, to_apply=%region_4.5 | all-reduce | flops 768 | bytes 6144 | tf_op jit(solution)/shard_map/psum | solution.py:39
  19.2 2.3 reduce-window.6
  21.5 0.3 slice_reduce_fusion
  21.7 0.2 eq.25
  22.1 0.2 copy.31
  22.3 0.3 mul.67
  22.6 0.2 fusion.7
  22.9 0.9 copy-done
  23.7 0.8 broadcast_in_dim.5
  24.5 0.6 reshape.110
  25.4 9.5 %scatter_custom_fusion = bf16[3072,512]{1,0:T(8,128)(2,1)} fusion(s32[1536]{0:T(1024)S(1)} %fusion.21, bf16[1536,512]{1,0:T(8,128)(2,1)S(1)} %reshape.110, bf16[]{:T(256)} %constant.8.clone.1), kind=kCustom, calls=%fused_computation.19 | custom fusion | bytes 3145730 | tf_op jit(solution)/shard_map/scatter | solution.py:52
  34.9 6.0 %all-to-all-start = ((bf16[8,384,512]{2,1,0:T(8,128)(2,1)}), bf16[8,384,512]{2,1,0:T(8,128)(2,1)}, u32[]{:S(2)}, u32[]{:S(2)}) async-start(bf16[8,384,512]{2,1,0:T(8,128)(2,1)} %bitcast.1), calls=%async_computation | async-start | bytes 6291456 | tf_op jit(solution)/shard_map/all_to_all | solution.py:60
  40.9 8.7 %all_gather.22 = bf16[1024,256]{1,0:T(8,128)(2,1)} all-gather(bf16[256,256]{1,0:T(8,128)(2,1)S(1)} %copy-done.2), channel_id=1, replica_groups=mesh['ep'=8,'tp'=4] {'tp'}, dimensions={0}, use_global_device_ids=true | all-gather | bytes 655360 | tf_op jit(solution)/shard_map/all_gather | solution.py:82
  49.6 75.0 %all-to-all-done = bf16[8,384,512]{2,1,0:T(8,128)(2,1)} async-done(((bf16[8,384,512]{2,1,0:T(8,128)(2,1)}), bf16[8,384,512]{2,1,0:T(8,128)(2,1)}, u32[]{:S(2)}, u32[]{:S(2)}) %all-to-all-start) | async-done | bytes 3145760 | tf_op jit(solution)/shard_map/all_to_all | solution.py:60
  124.6 3.7 all-to-all-start.1
  128.5 36.8 %all-to-all-done.1 = bf16[8,384,512]{2,1,0:T(8,128)(2,1)S(1)} async-done(((bf16[8,384,512]{2,1,0:T(8,128)(2,1)}), bf16[8,384,512]{2,1,0:T(8,128)(2,1)S(1)}, u32[]{:S(2)}, u32[]{:S(2)}) %all-to-all-start.1) | async-done | bytes 3145760 | tf_op jit(solution)/shard_map/all_to_all | solution.py:59
  165.2 0.9 stack.2
  166.1 4.3 %all-to-all-start.5 = ((bf16[4,256,256]{1,2,0:T(8,128)(2,1)}), bf16[4,256,256]{1,2,0:T(8,128)(2,1)}, u32[]{:S(2)}, u32[]{:S(2)}) async-start(bf16[4,256,256]{1,2,0:T(8,128)(2,1)} %stack.2), calls=%async_computation.5 | async-start | bytes 1048576 | tf_op jit(solution)/shard_map/all_to_all | solution.py:28
  170.4 2.4 copy.34
  172.8 1.0 copy.44
  173.9 4.6 %fusion.3 = f32[768,512]{1,0:T(8,128)} fusion(bf16[768,2048]{1,0:T(8,128)(2,1)S(1)} %bitcast.75, bf16[1,2048,512]{2,1,0:T(8,128)(2,1)} %all-gather.13.cloned.1.call-done), kind=kOutput, calls=%fused_computation.8 | convolution fusion | flops 1610612736 | bytes 6815744 | tf_op jit(solution)/shard_map/dot_general | solution.py:67
  178.5 7.9 %convolution_convert_fusion = bf16[768,2048]{1,0:T(8,128)(2,1)} fusion(bf16[1,512,2048]{2,1,0:T(8,128)(2,1)} %all-gather.17.cloned.1.call-done, f32[768,512]{1,0:T(8,128)} %fusion.3, bf16[768,2048]{1,0:T(8,128)(2,1)S(1)} %bitcast.76, bf16[1,2048,512]{2,1,0:T(8,128)(2,1)} %all-gather.15.cloned.1.call-done), kind=kOutput, calls=%fused_computation.2 | convolution fusion | flops 3225157632 | bytes 12058624 | tf_op jit(solution)/shard_map/dot_general | solution.py:70
  186.4 8.9 %copy.35 = bf16[2,384,2048]{1,0,2:T(2,128)(2,1)} copy(bf16[2,384,2048]{2,1,0:T(8,128)(2,1)} %bitcast.77) | data formatting | bytes 6291456 | tf_op jit(solution)/shard_map/reshape | solution.py:72
  195.3 3.7 all-to-all-start.2
  199.0 0.5 all-gather.9.cloned.1.call-update
  199.6 36.3 %all-to-all-done.2 = bf16[2,384,2048]{1,0,2:T(2,128)(2,1)S(1)} async-done(((bf16[2,384,2048]{1,0,2:T(2,128)(2,1)}), bf16[2,384,2048]{1,0,2:T(2,128)(2,1)S(1)}, u32[]{:S(2)}, u32[]{:S(2)}) %all-to-all-start.2) | async-done | bytes 3145760 | tf_op jit(solution)/shard_map/all_to_all | solution.py:71
  235.9 4.2 %all-to-all-start.4 = ((bf16[4,192,512]{2,1,0:T(8,128)(2,1)}), bf16[4,192,512]{2,1,0:T(8,128)(2,1)}, u32[]{:S(2)}, u32[]{:S(2)}) async-start(bf16[4,192,512]{2,1,0:T(8,128)(2,1)} %bitcast.74), calls=%async_computation.4 | async-start | bytes 1572864 | tf_op jit(solution)/shard_map/all_to_all | solution.py:79
  240.1 6.7 %copy.36 = bf16[4,2,384,512]{3,2,1,0:T(8,128)(2,1)} copy(bf16[4,2,384,512]{2,1,3,0:T(2,128)(2,1)S(1)} %bitcast.71) | data formatting | bytes 6291456 | tf_op jit(solution)/shard_map/all_to_all | solution.py:71
  246.8 5.0 %all-to-all-done.4 = bf16[4,192,512]{2,1,0:T(8,128)(2,1)} async-done(((bf16[4,192,512]{2,1,0:T(8,128)(2,1)}), bf16[4,192,512]{2,1,0:T(8,128)(2,1)}, u32[]{:S(2)}, u32[]{:S(2)}) %all-to-all-start.4) | async-done | bytes 786464 | tf_op jit(solution)/shard_map/all_to_all | solution.py:79
  251.7 6.3 %all-to-all-start.3 = ((bf16[8,384,512]{2,1,0:T(8,128)(2,1)}), bf16[8,384,512]{2,1,0:T(8,128)(2,1)S(1)}, u32[]{:S(2)}, u32[]{:S(2)}) async-start(bf16[8,384,512]{2,1,0:T(8,128)(2,1)} %bitcast.70), calls=%async_computation.3 | async-start | bytes 6291456 | tf_op jit(solution)/shard_map/all_to_all | solution.py:11
  258.0 2.1 copy.42
  260.1 41.1 %all-gather.9.cloned.1.call-done = bf16[2048,1024]{0,1:T(8,128)(2,1)} async-done(((bf16[256,1024]{0,1:T(8,128)(2,1)}), bf16[2048,1024]{0,1:T(8,128)(2,1)}) %all-gather.9.cloned.1.call-update) | async-done | bytes 4194320 | tf_op jit(solution)/shard_map/all_gather | solution.py:85
  301.2 7.0 %convolution_convert_fusion.1 = bf16[192,2048]{1,0:T(8,128)(2,1)} fusion(bf16[1024,2048]{1,0:T(8,128)(2,1)} %all-gather.11.cloned.1.call-done, bf16[192,2048]{1,0:T(8,128)(2,1)} %bitcast.79, bf16[2048,1024]{0,1:T(8,128)(2,1)} %all-gather.9.cloned.1.call-done), kind=kOutput, calls=%fused_computation.4 | convolution fusion | flops 1611988992 | bytes 9961472 | tf_op jit(solution)/shard_map/dot_general | solution.py:91
  308.2 2.1 copy.47
  310.3 33.7 %all-to-all-done.3 = bf16[8,384,512]{2,1,0:T(8,128)(2,1)S(1)} async-done(((bf16[8,384,512]{2,1,0:T(8,128)(2,1)}), bf16[8,384,512]{2,1,0:T(8,128)(2,1)S(1)}, u32[]{:S(2)}, u32[]{:S(2)}) %all-to-all-start.3) | async-done | bytes 3145760 | tf_op jit(solution)/shard_map/all_to_all | solution.py:11
  344.0 4.4 %all-to-all-start.6 = ((bf16[192,4,512]{2,0,1:T(8,128)(2,1)}), bf16[192,4,512]{2,0,1:T(8,128)(2,1)}, u32[]{:S(2)}, u32[]{:S(2)}) async-start(bf16[192,4,512]{2,0,1:T(8,128)(2,1)} %bitcast.78), calls=%async_computation.6 | async-start | bytes 1572864 | tf_op jit(solution)/shard_map/all_to_all | solution.py:94
  348.4 0.6 add_divide_fusion
  349.2 5.4 %gather_fusion = bf16[1536,512]{1,0:T(8,128)(2,1)} fusion(bf16[3072,512]{1,0:T(8,128)(2,1)S(1)} %bitcast.69, s32[2048]{0:T(1024)S(1)} %pad_clamp_fusion), kind=kCustom, calls=%fused_computation | custom fusion | bytes 3151872 | tf_op jit(solution)/shard_map/gather | solution.py:75
  354.6 3.4 reshape.96
  358.1 5.9 %multiply_reduce_fusion = f32[768,512]{1,0:T(8,128)} fusion(f32[768,2,512]{2,1,0:T(2,128)S(1)} %reshape.96, f32[768,2]{1,0:T(8,128)S(1)} %copy.37), kind=kLoop, calls=%fused_computation.3 | loop fusion | flops 1179648 | bytes 4724736 | tf_op jit(solution)/shard_map/reduce_sum | solution.py:78
  364.0 2.7 fusion.9
  (36 shorter events, 0.8 us)
Async XLA Ops:
  6.5 4.0 %copy-start.1 = (bf16[768,512]{1,0:T(8,128)(2,1)S(1)}, bf16[768,512]{1,0:T(8,128)(2,1)}, u32[]{:S(2)}) copy-start(bf16[768,512]{1,0:T(8,128)(2,1)} %param.10) | copy-start | bytes 2359300
  6.5 167.3 %all-gather.13.cloned.1.call-start = ((), (), s32[]{:S(2)}) async-start(), calls=%async_computation.9 | async-start | bytes 2621440 | tf_op jit(solution)/shard_map/all_gather | solution.py:55
  7.3 15.3 %copy-start.6 = (f32[512]{0:T(512)S(1)}, f32[512]{0:T(512)}, u32[]{:S(2)}) copy-start(f32[512]{0:T(512)} %param.11) | copy-start | bytes 6148
  7.3 171.3 %all-gather.15.cloned.1.call-start = ((), (), s32[]{:S(2)}) async-start(), calls=%async_computation.10 | async-start | bytes 2621440 | tf_op jit(solution)/shard_map/all_gather | solution.py:56
  8.0 170.5 %all-gather.17.cloned.1.call-start = ((), (), s32[]{:S(2)}) async-start(), calls=%async_computation.11 | async-start | bytes 2621440 | tf_op jit(solution)/shard_map/all_gather | solution.py:57
  22.9 0.9 copy-start
  34.9 6.0 %copy-start.2 = (bf16[256,256]{1,0:T(8,128)(2,1)S(1)}, bf16[256,256]{1,0:T(8,128)(2,1)}, u32[]{:S(2)}) copy-start(bf16[256,256]{1,0:T(8,128)(2,1)} %param.18) | copy-start | bytes 393220
  34.9 89.8 %all-to-all-start = ((bf16[8,384,512]{2,1,0:T(8,128)(2,1)}), bf16[8,384,512]{2,1,0:T(8,128)(2,1)}, u32[]{:S(2)}, u32[]{:S(2)}) async-start(bf16[8,384,512]{2,1,0:T(8,128)(2,1)} %bitcast.1), calls=%async_computation | async-start | bytes 6291456 | tf_op jit(solution)/shard_map/all_to_all | solution.py:60
  40.8 219.3 %all-gather.11.cloned.1.call-start = ((), (), s32[]{:S(2)}) async-start(), calls=%async_computation.8 | async-start | bytes 4718592 | tf_op jit(solution)/shard_map/all_gather | solution.py:86
  49.6 78.8 %copy-start.3 = (bf16[256,256]{1,0:T(8,128)(2,1)S(1)}, bf16[256,256]{1,0:T(8,128)(2,1)}, u32[]{:S(2)}) copy-start(bf16[256,256]{1,0:T(8,128)(2,1)} %param.17) | copy-start | bytes 393220
  124.6 40.6 %all-to-all-start.1 = ((bf16[8,384,512]{2,1,0:T(8,128)(2,1)}), bf16[8,384,512]{2,1,0:T(8,128)(2,1)S(1)}, u32[]{:S(2)}, u32[]{:S(2)}) async-start(bf16[8,384,512]{2,1,0:T(8,128)(2,1)} %all-to-all-done), calls=%async_computation.1 | async-start | bytes 6291456 | tf_op jit(solution)/shard_map/all_to_all | solution.py:59
  166.1 29.2 %all-to-all-start.5 = ((bf16[4,256,256]{1,2,0:T(8,128)(2,1)}), bf16[4,256,256]{1,2,0:T(8,128)(2,1)}, u32[]{:S(2)}, u32[]{:S(2)}) async-start(bf16[4,256,256]{1,2,0:T(8,128)(2,1)} %stack.2), calls=%async_computation.5 | async-start | bytes 1048576 | tf_op jit(solution)/shard_map/all_to_all | solution.py:28
  195.3 40.6 %all-to-all-start.2 = ((bf16[2,384,2048]{1,0,2:T(2,128)(2,1)}), bf16[2,384,2048]{1,0,2:T(2,128)(2,1)S(1)}, u32[]{:S(2)}, u32[]{:S(2)}) async-start(bf16[2,384,2048]{1,0,2:T(2,128)(2,1)} %copy.35), calls=%async_computation.2 | async-start | bytes 6291456 | tf_op jit(solution)/shard_map/all_to_all | solution.py:71
  199.0 102.2 %all-gather.9.cloned.1.call-start = ((), (), s32[]{:S(2)}) async-start(), calls=%async_computation.7 | async-start | bytes 4718592 | tf_op jit(solution)/shard_map/all_gather | solution.py:85
  235.9 15.9 %all-to-all-start.4 = ((bf16[4,192,512]{2,1,0:T(8,128)(2,1)}), bf16[4,192,512]{2,1,0:T(8,128)(2,1)}, u32[]{:S(2)}, u32[]{:S(2)}) async-start(bf16[4,192,512]{2,1,0:T(8,128)(2,1)} %bitcast.74), calls=%async_computation.4 | async-start | bytes 1572864 | tf_op jit(solution)/shard_map/all_to_all | solution.py:79
  251.7 92.3 %all-to-all-start.3 = ((bf16[8,384,512]{2,1,0:T(8,128)(2,1)}), bf16[8,384,512]{2,1,0:T(8,128)(2,1)S(1)}, u32[]{:S(2)}, u32[]{:S(2)}) async-start(bf16[8,384,512]{2,1,0:T(8,128)(2,1)} %bitcast.70), calls=%async_computation.3 | async-start | bytes 6291456 | tf_op jit(solution)/shard_map/all_to_all | solution.py:11
  308.2 40.2 %copy-start.7 = (f32[512]{0:T(512)S(1)}, f32[512]{0:T(512)}, u32[]{:S(2)}) copy-start(f32[512]{0:T(512)} %param.19) | copy-start | bytes 6148
  308.2 40.8 %copy-start.5 = (f32[768,2]{0,1:T(2,128)S(1)}, f32[768,2]{0,1:T(2,128)}, u32[]{:S(2)}) copy-start(f32[768,2]{0,1:T(2,128)} %param.13) | copy-start | bytes 18436
  344.0 20.0 %all-to-all-start.6 = ((bf16[192,4,512]{2,0,1:T(8,128)(2,1)}), bf16[192,4,512]{2,0,1:T(8,128)(2,1)}, u32[]{:S(2)}, u32[]{:S(2)}) async-start(bf16[192,4,512]{2,0,1:T(8,128)(2,1)} %bitcast.78), calls=%async_computation.6 | async-start | bytes 1572864 | tf_op jit(solution)/shard_map/all_to_all | solution.py:94
  358.1 5.9 %copy-start.4 = (f32[512]{0:T(512)S(1)}, f32[512]{0:T(512)}, u32[]{:S(2)}) copy-start(f32[512]{0:T(512)} %add_divide_fusion) | copy-start | bytes 6148
Sparse Core Ops, SparseCore 0:
  8.9 25.2 all-gather.12
  35.8 23.4 all-gather.14
  60.9 23.6 all-gather.16
  86.4 92.0 all-gather.10
  201.5 99.6 all-gather.8
